TPU v7x, 512 devices: a whole 4x8x8 slice. The times are simulated.
512 devices in a mesh: sp: 128 (over z, y, core), tp: 4 (over x).
Axes of the slice: x: 4, y: 8, z: 8, core: 2. Of those that a mesh axis runs over, the one named last changes fastest.
Arguments:
- tokens: bfloat16 [24576, 2048], P('sp'), may hold values from -10 to 10
- w_query: bfloat16 [2048, 1024], P(None, 'tp'), may hold values from -0.125 to 0.125
- w_key: bfloat16 [2048, 256], P(None, 'tp'), may hold values from -0.125 to 0.125
- w_value: bfloat16 [2048, 256], P(None, 'tp'), may hold values from -0.125 to 0.125
- w_output: bfloat16 [1024, 2048], P('tp'), may hold values from -0.1875 to 0.1875
- query_gain: float32 [64], replicated, may hold values from 0.4 to 9
- key_gain: float32 [64], replicated, may hold values from 0.4 to 9
Outputs:
- mixed_out: bfloat16 [24576, 2048], P(('sp', 'tp'))
- log_sums: float32 [16, 24576], P('tp', 'sp')
All inputs are finite; a program needn't handle non-finite values.
Results may differ from a plain program's by a relative error of at most 0.009.
The roundings to bfloat16 on the way count: a program that leaves them out, or rounds other values in their place, can miss the bound.
Values may be sent and summed in bfloat16 or wider, within the bound.
A program may use at most 64 MiB of HBM per device.

v0:
```python
import math
import jax
import jax.numpy as jnp
from jax import lax
from jax.sharding import PartitionSpec as P

GRID_W = 64
ROPE_BASE = 10000.0
NORM_EPS = 1e-06


def in_blocks(x, dim, peers):
    shape = x.shape
    tiles = x.reshape(*shape[:dim], peers, shape[dim] // peers, *shape[dim + 1 :])
    return jnp.moveaxis(tiles, dim, 0)


def sum_at_owner(x, axis, dim):
    tiles = in_blocks(x, dim, lax.axis_size(axis))
    arrived = lax.all_to_all(tiles, axis, split_axis=0, concat_axis=0, tiled=True)
    return arrived.sum(axis=0)


def rotate(values, position):
    dim = values.shape[-1]
    half_dim = dim // 2
    inverse = ROPE_BASE ** (-jnp.arange(half_dim, dtype=jnp.float32) * (2.0 / dim))
    angles = position.astype(jnp.float32)[:, None] * inverse[None, :]
    cosine = jnp.cos(angles)[:, None, :]
    sine = jnp.sin(angles)[:, None, :]
    first_half = values[..., :half_dim]
    second_half = values[..., half_dim:]
    return jnp.concatenate(
        [first_half * cosine - second_half * sine, second_half * cosine + first_half * sine], -1
    )


def prepare(projected, gain_vec, grid_row, grid_col):
    values = projected.astype(jnp.float32)
    values = values * lax.rsqrt(jnp.mean(values * values, -1, keepdims=True) + NORM_EPS) * gain_vec
    split_at = values.shape[-1] // 2
    turned = jnp.concatenate(
        [rotate(values[..., :split_at], grid_row), rotate(values[..., split_at:], grid_col)], -1
    )
    return turned.astype(jnp.bfloat16)


def shards(tokens, w_query, w_key, w_value, w_output, query_gain, key_gain):
    head_dim = query_gain.shape[0]
    n_query = w_query.shape[1]
    n_key = w_key.shape[1]
    combined = jnp.concatenate([w_query, w_key, w_value], axis=1)
    projected = jnp.dot(tokens, combined, preferred_element_type=jnp.float32).astype(jnp.bfloat16)
    seq_rows = projected.shape[0]
    local_heads = n_query // head_dim
    local_kv = n_key // head_dim
    group_size = local_heads // local_kv
    positions = lax.axis_index("sp") * seq_rows + jnp.arange(seq_rows, dtype=jnp.int32)
    grid_row = positions // GRID_W
    grid_col = positions % GRID_W
    queries = prepare(
        projected[:, :n_query].reshape(seq_rows, local_heads, head_dim),
        query_gain,
        grid_row,
        grid_col,
    )
    key_rows = prepare(
        projected[:, n_query : n_query + n_key].reshape(seq_rows, local_kv, head_dim),
        key_gain,
        grid_row,
        grid_col,
    )
    key_value = jnp.concatenate(
        [key_rows.reshape(seq_rows, n_key), projected[:, n_query + n_key :]], axis=1
    )
    grouped = queries.reshape(seq_rows, local_kv, group_size, head_dim).transpose(1, 2, 0, 3)
    grouped = grouped.reshape(local_kv, group_size * seq_rows, head_dim)
    score_scale = head_dim ** (-0.5)
    initial = (
        jnp.full((local_kv, group_size * seq_rows), -1e30, jnp.float32),
        jnp.zeros((local_kv, group_size * seq_rows), jnp.float32),
        jnp.zeros((local_kv, group_size * seq_rows, head_dim), jnp.float32),
    )
    gathered = lax.all_gather(key_value, "sp", axis=0, tiled=True)
    piece_rows = gathered.shape[0]
    span_rows = math.gcd(piece_rows, 1024)
    pieces = gathered.reshape(piece_rows // span_rows, span_rows, 2, local_kv, head_dim)

    def update(state, block):
        running, totals, weighted = state
        key_block = block[:, 0]
        value_block = block[:, 1]
        scores = (
            jnp.einsum("kqd,skd->kqs", grouped, key_block, preferred_element_type=jnp.float32)
            * score_scale
        )
        new_max = jnp.maximum(running, jnp.max(scores, -1))
        shrink = jnp.exp(running - new_max)
        expos = jnp.exp(scores - new_max[..., None])
        totals = totals * shrink + jnp.sum(expos, -1)
        weighted = weighted * shrink[..., None] + jnp.einsum(
            "kqs,skd->kqd",
            expos.astype(jnp.bfloat16),
            value_block,
            preferred_element_type=jnp.float32,
        )
        return ((new_max, totals, weighted), None)

    result, unused = lax.scan(update, initial, pieces)
    running, totals, weighted = result
    attended = (weighted / totals[..., None]).astype(jnp.bfloat16)
    attended = (
        attended.reshape(local_kv, group_size, seq_rows, head_dim)
        .transpose(2, 0, 1, 3)
        .reshape(seq_rows, n_query)
    )
    log_sums = (running + jnp.log(totals)).reshape(local_heads, seq_rows)
    mixed_out = sum_at_owner(
        jnp.dot(attended, w_output, preferred_element_type=jnp.float32), "tp", 0
    ).astype(jnp.bfloat16)
    return (mixed_out, log_sums)


def solution(mesh):
    placed = (P("sp", None), P(None, "tp"), P(None, "tp"), P(None, "tp"), P("tp", None), P(), P())
    return jax.shard_map(
        shards,
        mesh=mesh,
        in_specs=placed,
        out_specs=(P(("sp", "tp"), None), P("tp", "sp")),
        check_vma=False,
    )
```

profile of v0, /device:TPU:1, one launch (start us, length us, event | category | flops | bytes accessed | tf_op | source)
XLA Modules:
  0.0 347.7 jit_solution(5974512695529500345)
XLA Ops:
  7.3 1.3 copy.35
  8.6 1.2 copy.36
  9.8 2.3 fusion.25
  14.2 91.3 %all-gather.2.cloned.1.call-done = bf16[24576,128]{1,0:T(8,128)(2,1)} async-done(((bf16[192,128]{1,0:T(8,128)(2,1)}), bf16[24576,128]{1,0:T(8,128)(2,1)}) %all-gather.2.cloned.1.call-update) | async-done | bytes 6291472 | tf_op jit(solution)/shard_map/all_gather | solution.py:84
  105.5 21.6 %reshape.404 = bf16[24,1024,2,1,64]{4,2,1,0,3:T(2,128)(2,1)} reshape(bf16[24576,128]{1,0:T(8,128)(2,1)} %all-gather.2.cloned.1.call-done) | data formatting | bytes 12582912 | tf_op jit(solution)/shard_map/reshape | solution.py:87
  127.1 26.0 %copy.41 = bf16[24,1024,2,1,64]{1,4,3,2,0:T(8,128)(2,1)} copy(bf16[24,1024,2,1,64]{4,2,1,0,3:T(2,128)(2,1)} %reshape.404) | data formatting | bytes 12582912
  153.0 160.7 %while.15 = (s32[]{:T(128)}, f32[1,768]{1,0:T(1,128)S(1)}, f32[1,768]{1,0:T(1,128)S(1)}, f32[1,768,64]{1,2,0:T(8,128)S(1)}, bf16[24,1024,2,1,64]{1,4,3,2,0:T(8,1...) while((s32[]{:T(128)}, f32[1,768]{1,0:T(1,128)S(1)}, ...), condition=%wide.region_5.6_spmd.clone, body=%wide.region_2.5_spmd.clone.sunk | while | flops 207770112 | bytes 23450752 | solution.py:109
  154.0 2.3 multiply_reduce_fusion.2
  156.3 2.7 fusion.70
  159.7 1.0 dynamic-slice_bitcast_fusion.2
  160.7 2.3 multiply_reduce_fusion.2
  163.0 2.7 fusion.70
  166.4 1.0 dynamic-slice_bitcast_fusion.2
  167.4 2.3 multiply_reduce_fusion.2
  169.7 2.7 fusion.70
  173.1 1.0 dynamic-slice_bitcast_fusion.2
  174.1 2.3 multiply_reduce_fusion.2
  176.4 2.7 fusion.70
  179.8 1.0 dynamic-slice_bitcast_fusion.2
  180.8 2.3 multiply_reduce_fusion.2
  183.1 2.7 fusion.70
  186.5 1.0 dynamic-slice_bitcast_fusion.2
  187.5 2.3 multiply_reduce_fusion.2
  189.8 2.7 fusion.70
  193.2 1.0 dynamic-slice_bitcast_fusion.2
  194.2 2.3 multiply_reduce_fusion.2
  196.5 2.7 fusion.70
  200.9 2.3 multiply_reduce_fusion.2
  203.2 2.7 fusion.70
  207.6 2.3 multiply_reduce_fusion.2
  209.9 2.7 fusion.70
  214.2 2.3 multiply_reduce_fusion.2
  216.6 2.7 fusion.70
  220.9 2.3 multiply_reduce_fusion.2
  223.3 2.7 fusion.70
  227.6 2.3 multiply_reduce_fusion.2
  229.9 2.7 fusion.70
  234.3 2.3 multiply_reduce_fusion.2
  236.6 2.7 fusion.70
  241.0 2.3 multiply_reduce_fusion.2
  243.3 2.7 fusion.70
  247.7 2.3 multiply_reduce_fusion.2
  250.0 2.7 fusion.70
  254.4 2.3 multiply_reduce_fusion.2
  256.7 2.7 fusion.70
  261.1 2.3 multiply_reduce_fusion.2
  263.4 2.7 fusion.70
  267.8 2.3 multiply_reduce_fusion.2
  270.1 2.7 fusion.70
  274.5 2.3 multiply_reduce_fusion.2
  276.8 2.7 fusion.70
  281.2 2.3 multiply_reduce_fusion.2
  283.5 2.7 fusion.70
  287.9 2.3 multiply_reduce_fusion.2
  290.2 2.7 fusion.70
  294.6 2.3 multiply_reduce_fusion.2
  296.9 2.7 fusion.70
  301.3 2.3 multiply_reduce_fusion.2
  303.6 2.7 fusion.70
  308.0 2.3 multiply_reduce_fusion.2
  310.3 2.7 fusion.70
  314.3 1.5 fusion.28
  315.8 4.0 %all-to-all-start = ((f32[4,48,2048]{2,1,0:T(8,128)}), f32[4,48,2048]{2,1,0:T(8,128)S(1)}, u32[]{:S(2)}, u32[]{:S(2)}) async-start(f32[4,48,2048]{2,1,0:T(8,128)} %fusion.28), calls=%async_computation | async-start | bytes 3145728 | tf_op jit(solution)/shard_map/all_to_all | solution.py:20
  320.5 19.6 %all-to-all-done = f32[4,48,2048]{2,1,0:T(8,128)S(1)} async-done(((f32[4,48,2048]{2,1,0:T(8,128)}), f32[4,48,2048]{2,1,0:T(8,128)S(1)}, u32[]{:S(2)}, u32[]{:S(2)}) %all-to-all-start) | async-done | bytes 1572896 | tf_op jit(solution)/shard_map/all_to_all | solution.py:20
  (198 shorter events, 38.1 us)
Async XLA Ops:
  7.2 307.1 %copy-start = (bf16[256,2048]{1,0:T(8,128)(2,1)S(1)}, bf16[256,2048]{1,0:T(8,128)(2,1)}, u32[]{:S(2)}) copy-start(bf16[256,2048]{1,0:T(8,128)(2,1)} %param.13) | copy-start | bytes 3145732
  7.2 98.3 %all-gather.2.cloned.1.call-start = ((), (), s32[]{:S(2)}) async-start(), calls=%async_computation.1 | async-start | bytes 6340608 | tf_op jit(solution)/shard_map/all_gather | solution.py:84
  9.8 2.4 copy-start.2
  9.8 4.1 %copy-start.3 = (f32[64]{0:T(128)S(1)}, f32[64]{0:T(128)}, u32[]{:S(2)}) copy-start(f32[64]{0:T(128)} %param.14) | copy-start | bytes 772
  156.3 2.8 copy-start.1
  163.0 2.8 copy-start.1
  169.7 2.8 copy-start.1
  176.4 2.8 copy-start.1
  183.1 2.8 copy-start.1
  189.7 2.8 copy-start.1
  196.4 2.8 copy-start.1
  203.1 2.8 copy-start.1
  209.8 2.8 copy-start.1
  216.5 2.8 copy-start.1
  223.2 2.8 copy-start.1
  229.9 2.8 copy-start.1
  236.6 2.8 copy-start.1
  243.3 2.8 copy-start.1
  250.0 2.8 copy-start.1
  256.7 2.8 copy-start.1
  263.4 2.8 copy-start.1
  270.1 2.8 copy-start.1
  276.8 2.8 copy-start.1
  283.5 2.8 copy-start.1
  290.2 2.8 copy-start.1
  296.9 2.8 copy-start.1
  303.6 2.8 copy-start.1
  310.3 2.8 copy-start.1
  315.8 24.2 %all-to-all-start = ((f32[4,48,2048]{2,1,0:T(8,128)}), f32[4,48,2048]{2,1,0:T(8,128)S(1)}, u32[]{:S(2)}, u32[]{:S(2)}) async-start(f32[4,48,2048]{2,1,0:T(8,128)} %fusion.28), calls=%async_computation | async-start | bytes 3145728 | tf_op jit(solution)/shard_map/all_to_all | solution.py:20
Sparse Core Ops, SparseCore 0:
  13.7 91.7 all-gather.1
where the time goes:
time: 350 us; the launch traced here: 348 us
  matrix products  124 us (35%)
  waiting for transfers between devices  111 us (32%)
  local copies, waits for them, and re-layouts  77.4 us (22%)
  other arithmetic  16.5 us (5%)
  between operations  14.2 us (4%)
  starting transfers between devices  4 us (1%)
    all_gather x1, waiting for transfers between devices, shards(): gathered = lax.all_gather(key_value, 'sp', axis=0, tiled=True)  91.3 us
    dot_general x24, matrix products, update(): jnp.einsum('kqs,skd->kqd', expos.astype(jnp.bfloat16), value_block, prefe...  65.3 us
    dot_general x24, matrix products, update(): jnp.einsum('kqd,skd->kqs', grouped, key_block, preferred_element_type=jnp...  54.7 us
    unnamed x10, local copies, waits for them, and re-layouts  28.7 us
    squeeze x24, local copies, waits for them, and re-layouts, shards(): result, unused = lax.scan(update, initial, pieces)  23.3 us
    reshape x1, local copies, waits for them, and re-layouts, shards(): gathered.reshape(piece_rows // span_rows, span_rows, 2, local_kv, head_dim)  21.6 us
    all_to_all x1, waiting for transfers between devices, sum_at_owner(): lax.all_to_all(tiles, axis, split_axis=0, concat_axis=0, tiled=True)  19.6 us
    reduce_sum x24, other arithmetic, update(): totals = totals * shrink + jnp.sum(expos, -1)  13.4 us
  transfers between devices with their start and end apart: 2, of which 2 were waited for; matrix products, arithmetic and copies ran while one was open for 0% of the time, Pallas kernels for 0%

commit v1 on v0

--- a/solution.py
+++ b/solution.py
@@ -81,7 +81,9 @@
         jnp.zeros((local_kv, group_size * seq_rows), jnp.float32),
         jnp.zeros((local_kv, group_size * seq_rows, head_dim), jnp.float32),
     )
-    gathered = lax.all_gather(key_value, "sp", axis=0, tiled=True)
+    gathered = jnp.concatenate(
+        lax.all_to_all(jnp.stack([key_value] * lax.axis_size("sp")), "sp", 0, 0), axis=0
+    )
     piece_rows = gathered.shape[0]
     span_rows = math.gcd(piece_rows, 1024)
     pieces = gathered.reshape(piece_rows // span_rows, span_rows, 2, local_kv, head_dim)

time: 350 us -> 441 us (1.26)
  the two profiles are of different devices: /device:TPU:1 before, /device:TPU:17 now
where the time goes in v1:
time: 441 us; the launch traced here: 439 us
  waiting for transfers between devices  193 us (44%)
  matrix products  124 us (28%)
  local copies, waits for them, and re-layouts  81 us (18%)
  starting transfers between devices  22.1 us (5%)
  other arithmetic  16.5 us (4%)
    all_to_all x1, waiting for transfers between devices, shards(): lax.all_to_all(jnp.stack([key_value] * lax.axis_size('sp')), 'sp', 0, 0)  176 us
    dot_general x24, matrix products, update(): jnp.einsum('kqs,skd->kqd', expos.astype(jnp.bfloat16), value_block, prefe...  65.3 us
    dot_general x24, matrix products, update(): jnp.einsum('kqd,skd->kqs', grouped, key_block, preferred_element_type=jnp...  54.7 us
    unnamed x10, local copies, waits for them, and re-layouts  28.7 us
    squeeze x24, local copies, waits for them, and re-layouts, shards(): result, unused = lax.scan(update, initial, pieces)  23.3 us
    another operation x1, local copies, waits for them, and re-layouts, shards(): gathered.reshape(piece_rows // span_rows, span_rows, 2, local_kv, head_dim)  21.6 us
    all_to_all x1, starting transfers between devices, shards(): lax.all_to_all(jnp.stack([key_value] * lax.axis_size('sp')), 'sp', 0, 0)  18.1 us
    all_to_all x1, waiting for transfers between devices, sum_at_owner(): lax.all_to_all(tiles, axis, split_axis=0, concat_axis=0, tiled=True)  17.5 us
  transfers between devices with their start and end apart: 2, of which 2 were waited for; matrix products, arithmetic and copies ran while one was open for 0% of the time, Pallas kernels for 0%

profile of v1, /device:TPU:17, one launch (start us, length us, event | category | flops | bytes accessed | tf_op | source)
XLA Modules:
  0.0 438.5 jit_solution(3904720473924441146)
XLA Ops:
  0.7 1.3 copy.35
  2.0 1.2 copy.36
  3.2 2.3 fusion.25
  6.4 4.2 stack.2
  10.6 18.1 %all-to-all-start = ((bf16[128,192,128]{2,1,0:T(8,128)(2,1)}), bf16[128,192,128]{2,1,0:T(8,128)(2,1)}, u32[]{:S(2)}, u32[]{:S(2)}) async-start(bf16[128,192,128]{2,1,0:T(8,128)(2,1)} %stack.2), calls=%async_computation | async-start | bytes 12582912 | tf_op jit(solution)/shard_map/all_to_all | solution.py:85
  29.3 175.9 %all-to-all-done = bf16[128,192,128]{2,1,0:T(8,128)(2,1)} async-done(((bf16[128,192,128]{2,1,0:T(8,128)(2,1)}), bf16[128,192,128]{2,1,0:T(8,128)(2,1)}, u32[]{:S(2)}, u32[]{:S(2)}) %all-to-all-start) | async-done | bytes 6291488 | tf_op jit(solution)/shard_map/all_to_all | solution.py:85
  205.2 21.6 %reshape.402 = bf16[24,1024,2,1,64]{4,2,1,0,3:T(2,128)(2,1)} reshape(bf16[128,192,128]{2,1,0:T(8,128)(2,1)} %all-to-all-done) | data formatting | bytes 12582912 | tf_op jit(solution)/shard_map/reshape;reshape | solution.py:89
  226.8 26.0 %copy.41 = bf16[24,1024,2,1,64]{1,4,3,2,0:T(8,128)(2,1)} copy(bf16[24,1024,2,1,64]{4,2,1,0,3:T(2,128)(2,1)} %reshape.402) | data formatting | bytes 12582912
  252.7 160.7 %while.15 = (s32[]{:T(128)}, f32[1,768]{1,0:T(1,128)S(1)}, f32[1,768]{1,0:T(1,128)S(1)}, f32[1,768,64]{1,2,0:T(8,128)S(1)}, bf16[24,1024,2,1,64]{1,4,3,2,0:T(8,1...) while((s32[]{:T(128)}, f32[1,768]{1,0:T(1,128)S(1)}, ...), condition=%wide.region_5.6_spmd.clone, body=%wide.region_2.5_spmd.clone.sunk | while | flops 207770112 | bytes 23450752 | solution.py:111
  253.7 2.3 multiply_reduce_fusion.2
  256.0 2.7 fusion.70
  259.4 1.0 dynamic-slice_bitcast_fusion.2
  260.4 2.3 multiply_reduce_fusion.2
  262.7 2.7 fusion.70
  266.1 1.0 dynamic-slice_bitcast_fusion.2
  267.1 2.3 multiply_reduce_fusion.2
  269.4 2.7 fusion.70
  272.8 1.0 dynamic-slice_bitcast_fusion.2
  273.8 2.3 multiply_reduce_fusion.2
  276.1 2.7 fusion.70
  279.5 1.0 dynamic-slice_bitcast_fusion.2
  280.5 2.3 multiply_reduce_fusion.2
  282.8 2.7 fusion.70
  287.2 2.3 multiply_reduce_fusion.2
  289.5 2.7 fusion.70
  293.9 2.3 multiply_reduce_fusion.2
  296.2 2.7 fusion.70
  300.6 2.3 multiply_reduce_fusion.2
  302.9 2.7 fusion.70
  307.3 2.3 multiply_reduce_fusion.2
  309.6 2.7 fusion.70
  313.9 2.3 multiply_reduce_fusion.2
  316.3 2.7 fusion.70
  320.6 2.3 multiply_reduce_fusion.2
  322.9 2.7 fusion.70
  327.3 2.3 multiply_reduce_fusion.2
  329.6 2.7 fusion.70
  334.0 2.3 multiply_reduce_fusion.2
  336.3 2.7 fusion.70
  340.7 2.3 multiply_reduce_fusion.2
  343.0 2.7 fusion.70
  347.4 2.3 multiply_reduce_fusion.2
  349.7 2.7 fusion.70
  354.1 2.3 multiply_reduce_fusion.2
  356.4 2.7 fusion.70
  360.8 2.3 multiply_reduce_fusion.2
  363.1 2.7 fusion.70
  367.5 2.3 multiply_reduce_fusion.2
  369.8 2.7 fusion.70
  374.2 2.3 multiply_reduce_fusion.2
  376.5 2.7 fusion.70
  380.9 2.3 multiply_reduce_fusion.2
  383.2 2.7 fusion.70
  387.6 2.3 multiply_reduce_fusion.2
  389.9 2.7 fusion.70
  394.3 2.3 multiply_reduce_fusion.2
  396.6 2.7 fusion.70
  401.0 2.3 multiply_reduce_fusion.2
  403.3 2.7 fusion.70
  407.7 2.3 multiply_reduce_fusion.2
  410.0 2.7 fusion.70
  414.0 1.5 fusion.28
  415.5 4.0 all-to-all-start.1
  420.2 17.5 %all-to-all-done.1 = f32[4,48,2048]{2,1,0:T(8,128)S(1)} async-done(((f32[4,48,2048]{2,1,0:T(8,128)}), f32[4,48,2048]{2,1,0:T(8,128)S(1)}, u32[]{:S(2)}, u32[]{:S(2)}) %all-to-all-start.1) | async-done | bytes 1572896 | tf_op jit(solution)/shard_map/all_to_all | solution.py:20
  (198 shorter events, 39.3 us)
Async XLA Ops:
  0.6 413.4 %copy-start = (bf16[256,2048]{1,0:T(8,128)(2,1)S(1)}, bf16[256,2048]{1,0:T(8,128)(2,1)}, u32[]{:S(2)}) copy-start(bf16[256,2048]{1,0:T(8,128)(2,1)} %param.13) | copy-start | bytes 3145732
  3.2 2.3 copy-start.2
  10.6 18.4 %copy-start.3 = (f32[64]{0:T(128)S(1)}, f32[64]{0:T(128)}, u32[]{:S(2)}) copy-start(f32[64]{0:T(128)} %param.14) | copy-start | bytes 772
  10.6 194.6 %all-to-all-start = ((bf16[128,192,128]{2,1,0:T(8,128)(2,1)}), bf16[128,192,128]{2,1,0:T(8,128)(2,1)}, u32[]{:S(2)}, u32[]{:S(2)}) async-start(bf16[128,192,128]{2,1,0:T(8,128)(2,1)} %stack.2), calls=%async_computation | async-start | bytes 12582912 | tf_op jit(solution)/shard_map/all_to_all | solution.py:85
  256.0 2.8 copy-start.1
  262.7 2.8 copy-start.1
  269.4 2.8 copy-start.1
  276.1 2.8 copy-start.1
  282.8 2.8 copy-start.1
  289.4 2.8 copy-start.1
  296.1 2.8 copy-start.1
  302.8 2.8 copy-start.1
  309.5 2.8 copy-start.1
  316.2 2.8 copy-start.1
  322.9 2.8 copy-start.1
  329.6 2.8 copy-start.1
  336.3 2.8 copy-start.1
  343.0 2.8 copy-start.1
  349.7 2.8 copy-start.1
  356.4 2.8 copy-start.1
  363.1 2.8 copy-start.1
  369.8 2.8 copy-start.1
  376.5 2.8 copy-start.1
  383.2 2.8 copy-start.1
  389.9 2.8 copy-start.1
  396.6 2.8 copy-start.1
  403.3 2.8 copy-start.1
  410.0 2.8 copy-start.1
  415.5 22.2 %all-to-all-start.1 = ((f32[4,48,2048]{2,1,0:T(8,128)}), f32[4,48,2048]{2,1,0:T(8,128)S(1)}, u32[]{:S(2)}, u32[]{:S(2)}) async-start(f32[4,48,2048]{2,1,0:T(8,128)} %fusion.28), calls=%async_computation.1 | async-start | bytes 3145728 | tf_op jit(solution)/shard_map/all_to_all | solution.py:20
